TPU v7x, 32 devices: a whole 2x2x4 slice. The times are simulated.
32 devices in a mesh: fs: 8 (over z, core), tp: 4 (over y, x).
Axes of the slice: x: 2, y: 2, z: 4, core: 2. Of those that a mesh axis runs over, the one named last changes fastest.
Arguments:
- attn_out: bfloat16 [12288, 2048], P('fs', 'tp'), may hold values from -6 to 6
- out_cot: bfloat16 [12288, 4096], P('fs', 'tp'), may hold values from -6 to 6
- latent: bfloat16 [12288, 1024], P('fs', 'tp'), may hold values from -6 to 6
- value_cot: bfloat16 [12288, 2048], P('fs', 'tp'), may hold values from -6 to 6
- out_weight: float32 [2048, 4096], P('fs', 'tp'), may hold values from -0.125 to 0.125
- value_up_matrix: float32 [1024, 2048], P('fs', 'tp'), may hold values from -0.1875 to 0.1875
- out_basis: bfloat16 [2048, 256], P('fs'), as said below
- value_basis: bfloat16 [1024, 256], P('fs'), as said below
- out_mean: float32 [256, 4096], P(None, 'tp'), may hold values from -2660.43 to 2660.43
- out_square: float32 [256, 4096], P(None, 'tp'), may hold values from 12288 to 2457600, as said below
- value_mean: float32 [256, 2048], P(None, 'tp'), may hold values from -2660.43 to 2660.43
- value_square: float32 [256, 2048], P(None, 'tp'), may hold values from 12288 to 2457600, as said below
Outputs:
- out_step: float32 [2048, 4096], P('fs', 'tp')
- out_new: float32 [2048, 4096], P('fs', 'tp')
- out_copy: bfloat16 [2048, 4096], P(None, 'tp')
- out_mean_new: float32 [256, 4096], P(None, 'tp')
- out_square_new: float32 [256, 4096], P(None, 'tp')
- value_step: float32 [1024, 2048], P('fs', 'tp')
- value_new: float32 [1024, 2048], P('fs', 'tp')
- value_copy: bfloat16 [1024, 2048], P(None, 'tp')
- value_mean_new: float32 [256, 2048], P(None, 'tp')
- value_square_new: float32 [256, 2048], P(None, 'tp')
Inputs may be any that keep to these rules, and one draw needn't show every extreme that they name: `out_basis`: factors of full rank, rows of differing scales. `value_basis`: factors of full rank, rows of differing scales. `out_square`: Positive. `value_square`: Positive.
All inputs are finite; a program needn't handle non-finite values.
Results may differ from a plain program's by a relative error of at most 0.012.
Values may be sent and summed in bfloat16 or wider, within the bound.
A program may use at most 64 MiB of HBM per device.

v0:
```python
import jax
import jax.numpy as jnp
from jax import lax
from jax.sharding import PartitionSpec as P

LEARN_RATE = 0.01
MEAN_DECAY = 0.8
BETA_SQUARE = 0.9
EPS_RMS = 1e-06


def moments(proj, mean_in, square_in):
    mean_new = MEAN_DECAY * mean_in + (1.0 - MEAN_DECAY) * proj
    square_new = BETA_SQUARE * square_in + (1.0 - BETA_SQUARE) * proj * proj
    return (mean_new, square_new, mean_new / jnp.sqrt(square_new))


def split_product(lifted, cotangent):
    upper = lifted.astype(jnp.bfloat16)
    lower = (lifted - upper.astype(jnp.float32)).astype(jnp.bfloat16)
    first = jnp.dot(upper.T, cotangent, preferred_element_type=jnp.float32)
    return first + jnp.dot(lower.T, cotangent, preferred_element_type=jnp.float32)


def per_device(
    attn_out,
    out_cot,
    latent,
    value_cot,
    out_weight,
    value_up_matrix,
    out_basis,
    value_basis,
    out_mean,
    out_square,
    value_mean,
    value_square,
):
    width_out = out_cot.shape[1]
    head_cols = value_cot.shape[1]
    rows_out = out_basis.shape[0]
    rows_value = value_basis.shape[0]
    all_heads, all_latent = (
        lax.all_gather(attn_out, "tp", axis=1, tiled=True),
        lax.all_gather(latent, "tp", axis=1, tiled=True),
    )
    whole_o, whole_v = (
        lax.all_gather(out_basis, "fs", axis=0, tiled=True),
        lax.all_gather(value_basis, "fs", axis=0, tiled=True),
    )
    lifted_o = jnp.dot(all_heads, whole_o, preferred_element_type=jnp.float32)
    part_o = split_product(lifted_o, out_cot)
    lifted_v = jnp.dot(all_latent, whole_v, preferred_element_type=jnp.float32)
    part_v = split_product(lifted_v, value_cot)
    count_o = rows_out * lax.axis_size("fs") * width_out * lax.axis_size("tp")
    count_v = rows_value * lax.axis_size("fs") * head_cols * lax.axis_size("tp")
    proj_o, proj_v = (
        lax.psum(part_o.astype(jnp.bfloat16), "fs").astype(jnp.float32),
        lax.psum(part_v.astype(jnp.bfloat16), "fs").astype(jnp.float32),
    )
    mean_o, square_o, direction_o = moments(proj_o, out_mean, out_square)
    mean_v, square_v, direction_v = moments(proj_v, value_mean, value_square)
    update_o = jnp.dot(out_basis.astype(jnp.float32), direction_o, precision=lax.Precision.HIGHEST)
    update_v = jnp.dot(
        value_basis.astype(jnp.float32), direction_v, precision=lax.Precision.HIGHEST
    )
    total_o, total_v = lax.psum(
        (jnp.sum(update_o * update_o), jnp.sum(update_v * update_v)), ("fs", "tp")
    )
    step_o = LEARN_RATE * update_o * lax.rsqrt(total_o / count_o + EPS_RMS)
    step_v = LEARN_RATE * update_v * lax.rsqrt(total_v / count_v + EPS_RMS)
    new_o = out_weight - step_o
    new_v = value_up_matrix - step_v
    copy_o, copy_v = (
        lax.all_gather(new_o.astype(jnp.bfloat16), "fs", axis=0, tiled=True),
        lax.all_gather(new_v.astype(jnp.bfloat16), "fs", axis=0, tiled=True),
    )
    return (step_o, new_o, copy_o, mean_o, square_o, step_v, new_v, copy_v, mean_v, square_v)


def solution(mesh):
    placed = (
        P("fs", "tp"),
        P("fs", "tp"),
        P("fs", "tp"),
        P("fs", "tp"),
        P("fs", "tp"),
        P("fs", "tp"),
        P("fs", None),
        P("fs", None),
        P(None, "tp"),
        P(None, "tp"),
        P(None, "tp"),
        P(None, "tp"),
    )
    return jax.shard_map(
        per_device,
        mesh=mesh,
        in_specs=placed,
        out_specs=(
            P("fs", "tp"),
            P("fs", "tp"),
            P(None, "tp"),
            P(None, "tp"),
            P(None, "tp"),
            P("fs", "tp"),
            P("fs", "tp"),
            P(None, "tp"),
            P(None, "tp"),
            P(None, "tp"),
        ),
        check_vma=False,
    )
```

profile of v0, /device:TPU:0, one launch (start us, length us, event | category | flops | bytes accessed | tf_op | source)
XLA Modules:
  0.0 352.1 jit_solution(6366198598271107823)
XLA Ops:
  9.5 17.5 %all_gather.22 = bf16[1024,256]{1,0:T(8,128)(2,1)} all-gather(bf16[128,256]{1,0:T(8,128)(2,1)S(1)} %copy-done.11), channel_id=1, replica_groups=mesh['fs'=8,'tp'=4] {'fs'}, dimensions={0}, use_global_device_ids=true | all-gather | bytes 589824 | tf_op jit(solution)/shard_map/all_gather | solution.py:49
  27.0 29.3 %all-gather.12.cloned.1.call-done = bf16[1536,1024]{1,0:T(8,128)(2,1)} async-done(((bf16[1536,256]{1,0:T(8,128)(2,1)}), bf16[1536,1024]{1,0:T(8,128)(2,1)}) %all-gather.12.cloned.1.call-update) | async-done | bytes 3145744 | tf_op jit(solution)/shard_map/all_gather | solution.py:45
  56.3 3.1 fusion.21
  60.0 1.3 fusion.1
  61.3 18.8 %all-gather.8.cloned.1.call-done = bf16[2048,256]{1,0:T(8,128)(2,1)} async-done(((bf16[256,256]{1,0:T(8,128)(2,1)}), bf16[2048,256]{1,0:T(8,128)(2,1)}) %all-gather.8.cloned.1.call-update) | async-done | bytes 1048592 | tf_op jit(solution)/shard_map/all_gather | solution.py:48
  80.2 71.4 %all-gather.6.cloned.1.call-done = bf16[1536,2048]{1,0:T(8,128)(2,1)} async-done(((bf16[1536,512]{1,0:T(8,128)(2,1)}), bf16[1536,2048]{1,0:T(8,128)(2,1)}) %all-gather.6.cloned.1.call-update) | async-done | bytes 6291472 | tf_op jit(solution)/shard_map/all_gather | solution.py:44
  151.5 4.9 %fusion.20 = f32[1536,256]{1,0:T(8,128)S(1)} fusion(bf16[1536,2048]{1,0:T(8,128)(2,1)} %all-gather.6.cloned.1.call-done, bf16[2048,256]{1,0:T(8,128)(2,1)} %all-gather.8.cloned.1.call-done), kind=kOutput, calls=%fused_computation.32 | convolution fusion | flops 1610612736 | bytes 8912896 | tf_op jit(solution)/shard_map/dot_general | solution.py:51
  156.5 1.0 fusion.16
  157.5 1.8 fusion
  160.2 57.0 %all-reduce.4.cloned.1.call-done = (bf16[256,1024]{1,0:T(8,128)(2,1)}, bf16[256,512]{1,0:T(8,128)(2,1)}) async-done(((bf16[256,1024]{1,0:T(8,128)(2,1)}, bf16[256,512]{1,0:T(8,128)(2,1)}), (bf16[256,1024]{1,0:T(8,128)(2,1)}, bf16[256,512]{1,0:T(8,128)(2,1)})) %all-reduce.4.cloned.1.call-update) | async-done | bytes 786448 | tf_op jit(solution)/shard_map/psum | solution.py:58
  217.3 2.1 fusion.3
  219.4 2.6 multiply_reduce_fusion
  223.0 1.2 multiply_reduce_fusion.1
  224.2 39.5 %all-reduce = (f32[]{:T(128)}, f32[]{:T(128)}) all-reduce(f32[]{:T(128)} %get-tuple-element.34, f32[]{:T(128)} %get-tuple-element.36), channel_id=1, replica_groups=mesh['fs'=8,'tp'=4] {'fs','tp'}, use_global_device_ids=true, to_apply=%region_2.0 | all-reduce | flops 2 | bytes 16 | tf_op jit(solution)/shard_map/psum | solution.py:67
  264.4 1.8 fusion.18
  266.3 2.5 copy.22
  269.5 3.2 fusion.19
  272.8 2.6 copy.24
  275.4 2.6 copy.25
  277.9 1.8 copy.27
  280.6 9.7 %all-gather.14.cloned.1.call-done = bf16[1024,512]{0,1:T(8,128)(2,1)} async-done(((bf16[128,512]{0,1:T(8,128)(2,1)}), bf16[1024,512]{0,1:T(8,128)(2,1)}) %all-gather.14.cloned.1.call-update) | async-done | bytes 1048592 | tf_op jit(solution)/shard_map/all_gather | solution.py:76
  290.3 2.3 copy.29
  292.6 46.4 %all-gather.10.cloned.1.call-done = bf16[2048,1024]{0,1:T(8,128)(2,1)} async-done(((bf16[256,1024]{0,1:T(8,128)(2,1)}), bf16[2048,1024]{0,1:T(8,128)(2,1)}) %all-gather.10.cloned.1.call-update) | async-done | bytes 4194320 | tf_op jit(solution)/shard_map/all_gather | solution.py:75
  338.9 6.4 %copy.26 = bf16[2048,1024]{1,0:T(8,128)(2,1)} copy(bf16[2048,1024]{0,1:T(8,128)(2,1)} %all-gather.10.cloned.1.call-done) | data formatting | bytes 8388608
  (42 shorter events, 5.6 us)
Async XLA Ops:
  7.2 149.3 %copy-start = (bf16[1536,1024]{1,0:T(8,128)(2,1)S(1)}, bf16[1536,1024]{1,0:T(8,128)(2,1)}, u32[]{:S(2)}) copy-start(bf16[1536,1024]{1,0:T(8,128)(2,1)} %param.13) | copy-start | bytes 9437188
  7.2 2.3 copy-start.11
  7.2 49.1 %all-gather.12.cloned.1.call-start = ((), (), s32[]{:S(2)}) async-start(), calls=%async_computation.3 | async-start | bytes 3932160 | tf_op jit(solution)/shard_map/all_gather | solution.py:45
  7.9 72.2 %all-gather.8.cloned.1.call-start = ((), (), s32[]{:S(2)}) async-start(), calls=%async_computation.1 | async-start | bytes 1179648 | tf_op jit(solution)/shard_map/all_gather | solution.py:48
  8.7 142.8 %all-gather.6.cloned.1.call-start = ((), (), s32[]{:S(2)}) async-start(), calls=%async_computation | async-start | bytes 7864320 | tf_op jit(solution)/shard_map/all_gather | solution.py:44
  9.4 207.9 %all-reduce.4.cloned.1.call-start = ((), (), s32[]{:S(2)}) async-start(), calls=%async_computation.5 | async-start | bytes 1572864 | tf_op jit(solution)/shard_map/psum | solution.py:58
  56.3 3.1 copy-start.1
  157.5 1.9 copy-start.12
  159.3 130.9 %all-gather.14.cloned.1.call-start = ((), (), s32[]{:S(2)}) async-start(), calls=%async_computation.4 | async-start | bytes 1179648 | tf_op jit(solution)/shard_map/all_gather | solution.py:76
  217.3 2.1 copy-start.7
  219.3 2.7 copy-start.2
  219.4 2.7 copy-start.3
  219.4 2.6 copy-start.8
  219.4 2.6 copy-start.9
  219.4 2.6 copy-start.10
  222.2 0.8 copy-start.4
  222.2 2.0 copy-start.5
  266.3 72.6 %all-gather.10.cloned.1.call-start = ((), (), s32[]{:S(2)}) async-start(), calls=%async_computation.2 | async-start | bytes 4718592 | tf_op jit(solution)/shard_map/all_gather | solution.py:75
  275.4 4.4 %copy-start.6 = (f32[128,512]{0,1:T(8,128)S(1)}, f32[128,512]{0,1:T(8,128)}, u32[]{:S(2)}) copy-start(f32[128,512]{0,1:T(8,128)} %get-tuple-element.25) | copy-start | bytes 786436
Sparse Core Ops, SparseCore 0:
  9.8 46.4 all-gather.11
  57.9 22.2 all-gather.7
  82.0 69.4 all-gather.5
  159.5 57.7 all-reduce.3
  266.4 23.8 all-gather.13
  292.3 46.5 all-gather.9
where the time goes:
time: 353 us; the launch traced here: 352 us
  waiting for transfers between devices  235 us (67%)
  blocking collectives  57 us (16%)
  local copies, waits for them, and re-layouts  20.6 us (6%)
  matrix products  16.6 us (5%)
  between operations  15.7 us (4%)
  other arithmetic  7.29 us (2%)
    all_gather x1, waiting for transfers between devices, per_device(): lax.all_gather(attn_out, 'tp', axis=1, tiled=True)  71.4 us
    psum x1, waiting for transfers between devices, per_device(): lax.psum(part_o.astype(jnp.bfloat16), 'fs').astype(jnp.float32)  57 us
    all_gather x1, waiting for transfers between devices, per_device(): lax.all_gather(new_o.astype(jnp.bfloat16), 'fs', axis=0, tiled=True)  46.4 us
    psum x1, blocking collectives, per_device(): lax.psum((jnp.sum(update_o * update_o), jnp.sum(update_v * update_v)), ('...  39.5 us
    all_gather x1, waiting for transfers between devices, per_device(): lax.all_gather(latent, 'tp', axis=1, tiled=True)  29.3 us
    unnamed x34, local copies, waits for them, and re-layouts  20.6 us
    all_gather x1, waiting for transfers between devices, per_device(): lax.all_gather(out_basis, 'fs', axis=0, tiled=True)  18.8 us
    all_gather x1, blocking collectives, per_device(): lax.all_gather(value_basis, 'fs', axis=0, tiled=True)  17.5 us
  transfers between devices with their start and end apart: 6, of which 6 were waited for; matrix products, arithmetic and copies ran while one was open for 6% of the time, Pallas kernels for 0%

commit v1 on v0

--- a/solution.py
+++ b/solution.py
@@ -55,7 +55,7 @@
     count_o = rows_out * lax.axis_size("fs") * width_out * lax.axis_size("tp")
     count_v = rows_value * lax.axis_size("fs") * head_cols * lax.axis_size("tp")
     proj_o, proj_v = (
-        lax.psum(part_o.astype(jnp.bfloat16), "fs").astype(jnp.float32),
+        jnp.sum(lax.all_gather(part_o.astype(jnp.bfloat16), "fs"), axis=0).astype(jnp.float32),
         lax.psum(part_v.astype(jnp.bfloat16), "fs").astype(jnp.float32),
     )
     mean_o, square_o, direction_o = moments(proj_o, out_mean, out_square)

time: 353 us -> 395 us (1.12)
  waiting for transfers between devices: 235 us -> 272 us
  other arithmetic: 7.29 us -> 12.6 us
    all_gather x0 -> x1, waiting for transfers between devices: none -> 44.3 us  [per_device(): lax.all_gather(part_o.astype(jnp.bfloat16), 'fs')]
    psum x1, waiting for transfers between devices: 57 us -> 49.5 us  [per_device(): lax.psum(part_v.astype(jnp.bfloat16), 'fs').astype(jnp.float32)]
    reduce_sum x0 -> x1, other arithmetic: none -> 4 us  [per_device(): jnp.sum(lax.all_gather(part_o.astype(jnp.bfloat16), 'fs'), axis=0)]
    unnamed x34 -> x28, local copies, waits for them, and re-layouts: 20.6 us -> 20.8 us
  transfers between devices with their start and end apart: 6 -> 7, of which waited for: 6 -> 7; matrix products, arithmetic and copies ran while one was open for 6% -> 8% of each run, Pallas kernels for 0% -> 0%
where the time goes in v1:
time: 395 us; the launch traced here: 394 us
  waiting for transfers between devices  272 us (69%)
  blocking collectives  56.8 us (14%)
  local copies, waits for them, and re-layouts  20.8 us (5%)
  matrix products  16.5 us (4%)
  between operations  15.7 us (4%)
  other arithmetic  12.6 us (3%)
    all_gather x1, waiting for transfers between devices, per_device(): lax.all_gather(attn_out, 'tp', axis=1, tiled=True)  71.4 us
    psum x1, waiting for transfers between devices, per_device(): lax.psum(part_v.astype(jnp.bfloat16), 'fs').astype(jnp.float32)  49.5 us
    all_gather x1, waiting for transfers between devices, per_device(): lax.all_gather(new_o.astype(jnp.bfloat16), 'fs', axis=0, tiled=True)  46.5 us
    all_gather x1, waiting for transfers between devices, per_device(): lax.all_gather(part_o.astype(jnp.bfloat16), 'fs')  44.3 us
    psum x1, blocking collectives, per_device(): lax.psum((jnp.sum(update_o * update_o), jnp.sum(update_v * update_v)), ('...  39.2 us
    all_gather x1, waiting for transfers between devices, per_device(): lax.all_gather(latent, 'tp', axis=1, tiled=True)  29.3 us
    unnamed x28, local copies, waits for them, and re-layouts  20.8 us
    all_gather x1, waiting for transfers between devices, per_device(): lax.all_gather(out_basis, 'fs', axis=0, tiled=True)  18.8 us
  transfers between devices with their start and end apart: 7, of which 7 were waited for; matrix products, arithmetic and copies ran while one was open for 8% of the time, Pallas kernels for 0%

profile of v1, /device:TPU:0, one launch (start us, length us, event | category | flops | bytes accessed | tf_op | source)
XLA Modules:
  0.0 394.2 jit_solution(1463028151386565865)
XLA Ops:
  9.5 17.5 %all_gather.30 = bf16[1024,256]{1,0:T(8,128)(2,1)} all-gather(bf16[128,256]{1,0:T(8,128)(2,1)S(1)} %copy-done.8), channel_id=1, replica_groups=mesh['fs'=8,'tp'=4] {'fs'}, dimensions={0}, use_global_device_ids=true | all-gather | bytes 589824 | tf_op jit(solution)/shard_map/all_gather | solution.py:49
  27.0 29.3 %all-gather.14.cloned.1.call-done = bf16[1536,1024]{1,0:T(8,128)(2,1)} async-done(((bf16[1536,256]{1,0:T(8,128)(2,1)}), bf16[1536,1024]{1,0:T(8,128)(2,1)}) %all-gather.14.cloned.1.call-update) | async-done | bytes 3145744 | tf_op jit(solution)/shard_map/all_gather | solution.py:45
  56.3 3.1 fusion.21
  61.4 18.8 %all-gather.10.cloned.1.call-done = bf16[2048,256]{1,0:T(8,128)(2,1)} async-done(((bf16[256,256]{1,0:T(8,128)(2,1)}), bf16[2048,256]{1,0:T(8,128)(2,1)}) %all-gather.10.cloned.1.call-update) | async-done | bytes 1048592 | tf_op jit(solution)/shard_map/all_gather | solution.py:48
  80.2 71.4 %all-gather.8.cloned.1.call-done = bf16[1536,2048]{1,0:T(8,128)(2,1)} async-done(((bf16[1536,512]{1,0:T(8,128)(2,1)}), bf16[1536,2048]{1,0:T(8,128)(2,1)}) %all-gather.8.cloned.1.call-update) | async-done | bytes 6291472 | tf_op jit(solution)/shard_map/all_gather | solution.py:44
  151.5 4.9 %fusion.20 = f32[1536,256]{1,0:T(8,128)S(1)} fusion(bf16[1536,2048]{1,0:T(8,128)(2,1)} %all-gather.8.cloned.1.call-done, bf16[2048,256]{1,0:T(8,128)(2,1)} %all-gather.10.cloned.1.call-done), kind=kOutput, calls=%fused_computation.32 | convolution fusion | flops 1610612736 | bytes 8912896 | tf_op jit(solution)/shard_map/dot_general | solution.py:51
  157.5 1.8 fusion
  160.2 49.5 %all-reduce.3.cloned.1.call-done = bf16[256,512]{1,0:T(8,128)(2,1)} async-done(((bf16[256,512]{1,0:T(8,128)(2,1)}), bf16[256,512]{1,0:T(8,128)(2,1)}) %all-reduce.3.cloned.1.call-update) | async-done | bytes 262160 | tf_op jit(solution)/shard_map/psum | solution.py:59
  209.7 1.5 fusion.8
  213.3 44.3 %all-gather.18.cloned.1.call-done = bf16[2048,1024]{1,0:T(8,128)(2,1)} async-done(((bf16[256,1024]{1,0:T(8,128)(2,1)}), bf16[2048,1024]{1,0:T(8,128)(2,1)}) %all-gather.18.cloned.1.call-update) | async-done | bytes 4194320 | tf_op jit(solution)/shard_map/all_gather | solution.py:58
  257.7 4.0 %reduce_sum.30 = bf16[256,1024]{1,0:T(8,128)(2,1)} reduce(bf16[8,256,1024]{2,1,0:T(8,128)(2,1)} %bitcast.17, bf16[]{:T(256)} %constant.11.clone.1), dimensions={0}, to_apply=%region_0.0 | reduce | flops 1835008 | bytes 4718594 | tf_op jit(solution)/shard_map/reduce_sum | solution.py:58
  261.7 2.1 fusion.3
  263.8 2.6 multiply_reduce_fusion
  266.4 39.2 %all-reduce = (f32[]{:T(128)}, f32[]{:T(128)}) all-reduce(f32[]{:T(128)} %get-tuple-element.32, f32[]{:T(128)} %get-tuple-element.34), channel_id=1, replica_groups=mesh['fs'=8,'tp'=4] {'fs','tp'}, use_global_device_ids=true, to_apply=%region_2.0 | all-reduce | flops 2 | bytes 16 | tf_op jit(solution)/shard_map/psum | solution.py:67
  306.3 1.8 fusion.18
  308.2 2.5 copy.22
  311.4 3.2 fusion.19
  314.7 2.6 copy.24
  317.3 2.6 copy.25
  319.8 1.8 copy.27
  322.5 9.7 %all-gather.16.cloned.1.call-done = bf16[1024,512]{0,1:T(8,128)(2,1)} async-done(((bf16[128,512]{0,1:T(8,128)(2,1)}), bf16[1024,512]{0,1:T(8,128)(2,1)}) %all-gather.16.cloned.1.call-update) | async-done | bytes 1048592 | tf_op jit(solution)/shard_map/all_gather | solution.py:76
  332.1 2.3 copy.29
  334.4 46.5 %all-gather.12.cloned.1.call-done = bf16[2048,1024]{0,1:T(8,128)(2,1)} async-done(((bf16[256,1024]{0,1:T(8,128)(2,1)}), bf16[2048,1024]{0,1:T(8,128)(2,1)}) %all-gather.12.cloned.1.call-update) | async-done | bytes 4194320 | tf_op jit(solution)/shard_map/all_gather | solution.py:75
  380.9 6.4 %copy.26 = bf16[2048,1024]{1,0:T(8,128)(2,1)} copy(bf16[2048,1024]{0,1:T(8,128)(2,1)} %all-gather.12.cloned.1.call-done) | data formatting | bytes 8388608
  (40 shorter events, 9.2 us)
Async XLA Ops:
  7.2 149.3 %copy-start = (bf16[1536,1024]{1,0:T(8,128)(2,1)S(1)}, bf16[1536,1024]{1,0:T(8,128)(2,1)}, u32[]{:S(2)}) copy-start(bf16[1536,1024]{1,0:T(8,128)(2,1)} %param.13) | copy-start | bytes 9437188
  7.2 2.3 copy-start.8
  7.2 49.1 %all-gather.14.cloned.1.call-start = ((), (), s32[]{:S(2)}) async-start(), calls=%async_computation.3 | async-start | bytes 3932160 | tf_op jit(solution)/shard_map/all_gather | solution.py:45
  7.9 72.2 %all-gather.10.cloned.1.call-start = ((), (), s32[]{:S(2)}) async-start(), calls=%async_computation.1 | async-start | bytes 1179648 | tf_op jit(solution)/shard_map/all_gather | solution.py:48
  8.7 142.8 %all-gather.8.cloned.1.call-start = ((), (), s32[]{:S(2)}) async-start(), calls=%async_computation | async-start | bytes 7864320 | tf_op jit(solution)/shard_map/all_gather | solution.py:44
  9.4 200.3 %all-reduce.3.cloned.1.call-start = ((), (), s32[]{:S(2)}) async-start(), calls=%async_computation.4 | async-start | bytes 524288 | tf_op jit(solution)/shard_map/psum | solution.py:59
  56.3 3.1 copy-start.1
  61.4 196.3 %all-gather.18.cloned.1.call-start = ((), (), s32[]{:S(2)}) async-start(), calls=%async_computation.6 | async-start | bytes 4718592 | tf_op jit(solution)/shard_map/all_gather | solution.py:58
  157.5 1.9 copy-start.9
  159.3 172.8 %all-gather.16.cloned.1.call-start = ((), (), s32[]{:S(2)}) async-start(), calls=%async_computation.5 | async-start | bytes 1179648 | tf_op jit(solution)/shard_map/all_gather | solution.py:76
  211.2 0.8 copy-start.4
  211.2 1.0 copy-start.5
  261.7 2.1 copy-start.7
  263.8 2.6 copy-start.2
  263.8 2.6 copy-start.3
  308.2 72.8 %all-gather.12.cloned.1.call-start = ((), (), s32[]{:S(2)}) async-start(), calls=%async_computation.2 | async-start | bytes 4718592 | tf_op jit(solution)/shard_map/all_gather | solution.py:75
  317.3 4.4 %copy-start.6 = (f32[128,512]{0,1:T(8,128)S(1)}, f32[128,512]{0,1:T(8,128)}, u32[]{:S(2)}) copy-start(f32[128,512]{0,1:T(8,128)} %get-tuple-element.23) | copy-start | bytes 786436
Sparse Core Ops, SparseCore 0:
  9.8 46.4 all-gather.13
  57.9 22.2 all-gather.9
  82.0 69.4 all-gather.7
  154.3 55.4 all-reduce.2
  211.7 45.9 all-gather.17
  308.3 23.8 all-gather.15
  334.3 46.5 all-gather.11
